TPU v7x, 32 devices: a whole 2x2x4 slice. The times are simulated.
32 devices in a mesh: sp: 8 (over z, x), tp: 4 (over y, core).
Axes of the slice: x: 2, y: 2, z: 4, core: 2. Of those that a mesh axis runs over, the one named last changes fastest.
Arguments:
- tokens: bfloat16 [2, 128, 1024], P(None, 'sp', 'tp'), may hold values from -6 to 6
- in_weight: bfloat16 [3, 1024, 2048], P(None, 'sp', 'tp'), may hold values from -0.1875 to 0.1875
- gate_weight: bfloat16 [3, 1024, 2048], P(None, 'sp', 'tp'), may hold values from -0.1875 to 0.1875
- out_weight: bfloat16 [3, 2048, 1024], P(None, 'tp', 'sp'), may hold values from -0.25 to 0.25
- recur_weight: bfloat16 [3, 2, 16, 128, 128], P(None, None, 'tp'), may hold values from -0.5 to 0.5
- input_weight: bfloat16 [3, 2, 16, 128, 128], P(None, None, 'tp'), may hold values from -0.5 to 0.5
- conv_taps: bfloat16 [3, 4, 2048], P(None, None, 'tp'), may hold values from -3 to 3
- decay_rate: float32 [3, 2, 2048], P(None, None, 'tp'), may hold values from 0.02 to 0.25
- norm_gain: float32 [3, 1024], replicated, may hold values from 0.5 to 1.5
Outputs:
- mixed_out: bfloat16 [2, 128, 1024], P(None, 'sp', 'tp')
All inputs are finite; a program needn't handle non-finite values.
Results may differ from a plain program's by a relative error of at most 0.04.
Values may be sent and summed in bfloat16 or wider, within the bound.
A program may use at most 64 MiB of HBM per device.

v0:
```python
import jax
import jax.numpy as jnp
from jax import lax
from jax.sharding import PartitionSpec as P

LAYERS = 3
epsilon = 1e-06
gate_power = 8.0


def extended(array, sides, width, wrap):
    for axis, dim in sides:
        size, length = (lax.axis_size(axis), array.shape[dim])
        up = [(i, (i + 1) % size) for i in range(size if wrap else size - 1)]
        down = [(j, i) for i, j in up]
        last = lax.slice_in_dim(array, length - width, length, axis=dim)
        initial = lax.slice_in_dim(array, 0, width, axis=dim)
        before = lax.ppermute(last, axis, up)
        after = lax.ppermute(initial, axis, down)
        array = jnp.concatenate([before, array, after], axis=dim)
    return array


def carried_in(value, axis, join, neutral, backward):
    count, mine = (lax.axis_size(axis), lax.axis_index(axis))
    pieces = jax.tree.map(lambda part: lax.all_gather(part, axis), value)
    if backward:
        pieces = jax.tree.map(lambda part: part[::-1], pieces)
        mine = count - 1 - mine
    subtotal = jax.tree.map(
        lambda part, zero: jnp.full_like(part, 0) + jnp.asarray(zero, part.dtype), value, neutral
    )

    def hop(position, subtotal):
        longer = join(subtotal, jax.tree.map(lambda part: part[position], pieces))
        return jax.tree.map(lambda new, old: jnp.where(position < mine, new, old), longer, subtotal)

    return lax.fori_loop(0, count - 1, hop, subtotal)


def combine(earlier, later_pair):
    first_decay, first_drive = earlier
    second_decay, second_drive = later_pair
    return (first_decay * second_decay, second_decay * first_drive + second_drive)


def body(
    tokens,
    in_weight,
    gate_weight,
    out_weight,
    recur_weight,
    input_weight,
    conv_taps,
    decay_rate,
    norm_gain,
):
    batch_size, tok_rows, _ = tokens.shape
    seq_len = tok_rows * lax.axis_size("sp")
    chan_width = in_weight.shape[2]
    in_whole, gate_whole = (
        lax.all_gather(in_weight, "sp", axis=1, tiled=True),
        lax.all_gather(gate_weight, "sp", axis=1, tiled=True),
    )
    out_whole = lax.all_gather(out_weight, "sp", axis=2, tiled=True)
    state = tokens
    for layer_index in range(LAYERS):
        gathered = lax.all_gather(state, "tp", axis=2, tiled=True)
        flat_rows = gathered.reshape(batch_size * tok_rows, -1).astype(jnp.float32)
        scale_rows = lax.rsqrt(jnp.mean(flat_rows * flat_rows, axis=-1, keepdims=True) + epsilon)
        normed = (flat_rows * scale_rows * norm_gain[layer_index]).astype(jnp.bfloat16)
        branch = jnp.dot(normed, in_whole[layer_index], preferred_element_type=jnp.float32)
        gate_branch = jnp.dot(normed, gate_whole[layer_index], preferred_element_type=jnp.float32)
        branch = branch.astype(jnp.bfloat16).reshape(batch_size, tok_rows, chan_width)
        gate_branch = gate_branch.astype(jnp.bfloat16).reshape(batch_size, tok_rows, chan_width)
        padded = extended(branch, (("sp", 1),), 2, False)
        tap_values = conv_taps[layer_index].astype(jnp.float32)
        conv_out = padded[:, 0:tok_rows].astype(jnp.float32) * tap_values[0]
        for tap_index in range(1, tap_values.shape[0]):
            conv_out = (
                conv_out
                + padded[:, tap_index : tap_index + tok_rows].astype(jnp.float32)
                * tap_values[tap_index]
            )
        conv_out = conv_out.astype(jnp.bfloat16)
        conv_float = conv_out.astype(jnp.float32)
        recur_full = recur_weight[layer_index]
        input_full = input_weight[layer_index]
        heads_local = recur_full.shape[1]
        head_dim = recur_full.shape[2]
        blocks = conv_out.reshape(batch_size, tok_rows, heads_local, head_dim)
        hidden_sum = jnp.zeros((batch_size, tok_rows, chan_width), jnp.float32)
        identity = (
            jnp.ones((batch_size, chan_width), jnp.float32),
            jnp.zeros((batch_size, chan_width), jnp.float32),
        )
        for direction in range(2):
            recur_gate = jax.nn.sigmoid(
                jnp.einsum(
                    "bthd,hde->bthe",
                    blocks,
                    recur_full[direction],
                    preferred_element_type=jnp.float32,
                )
            ).reshape(batch_size, tok_rows, chan_width)
            input_gate = jax.nn.sigmoid(
                jnp.einsum(
                    "bthd,hde->bthe",
                    blocks,
                    input_full[direction],
                    preferred_element_type=jnp.float32,
                )
            ).reshape(batch_size, tok_rows, chan_width)
            log_decay = -gate_power * recur_gate * decay_rate[layer_index, direction] / seq_len
            decay_step = jnp.exp(log_decay)
            driven = jnp.sqrt(-jnp.expm1(2.0 * log_decay)) * input_gate * conv_float
            backward = direction == 1
            cum_decay, cum_drive = lax.associative_scan(
                combine, (decay_step, driven), axis=1, reverse=backward
            )
            if backward:
                totals = (cum_decay[:, 0], cum_drive[:, 0])
                incoming = carried_in(totals, "sp", combine, identity, True)
            else:
                totals = (cum_decay[:, -1], cum_drive[:, -1])
                incoming = carried_in(totals, "sp", combine, identity, False)
            hidden_sum = hidden_sum + (cum_decay * incoming[1][:, None, :] + cum_drive)
        mixed_rows = (hidden_sum * jax.nn.silu(gate_branch.astype(jnp.float32))).astype(
            jnp.bfloat16
        )
        mixed_rows = mixed_rows.reshape(batch_size * tok_rows, chan_width)
        partial_terms = jnp.dot(
            mixed_rows, out_whole[layer_index], preferred_element_type=jnp.float32
        )
        shard_sum = lax.psum_scatter(
            partial_terms.astype(jnp.bfloat16), "tp", scatter_dimension=1, tiled=True
        ).astype(jnp.float32)
        state = shard_sum.astype(jnp.bfloat16).reshape(batch_size, tok_rows, -1)
    return state


def solution(mesh):
    in_specs = (
        P(None, "sp", "tp"),
        P(None, "sp", "tp"),
        P(None, "sp", "tp"),
        P(None, "tp", "sp"),
        P(None, None, "tp", None, None),
        P(None, None, "tp", None, None),
        P(None, None, "tp"),
        P(None, None, "tp"),
        P(),
    )
    out_specs = P(None, "sp", "tp")
    return jax.shard_map(body, mesh=mesh, in_specs=in_specs, out_specs=out_specs, check_vma=False)
```

profile of v0, /device:TPU:0, one launch (start us, length us, event | category | flops | bytes accessed | tf_op | source)
XLA Modules:
  0.0 657.9 jit_solution(7241306334868398253)
XLA Ops:
  12.4 6.5 all_gather.54
  19.1 53.2 %all-gather.16.cloned.1.call-done = bf16[3,1024,512]{2,1,0:T(8,128)(2,1)} async-done(((bf16[3,128,512]{2,1,0:T(8,128)(2,1)}), bf16[3,1024,512]{2,1,0:T(8,128)(2,1)}) %all-gather.16.cloned.1.call-update) | async-done | bytes 3145744 | tf_op jit(solution)/shard_map/all_gather | solution.py:62
  75.1 4.5 collective-permute-start
  79.7 53.5 %all-gather.18.cloned.1.call-done = bf16[3,1024,512]{2,1,0:T(8,128)(2,1)} async-done(((bf16[3,128,512]{2,1,0:T(8,128)(2,1)}), bf16[3,1024,512]{2,1,0:T(8,128)(2,1)}) %all-gather.18.cloned.1.call-update) | async-done | bytes 3145744 | tf_op jit(solution)/shard_map/all_gather | solution.py:63
  138.2 30.9 %all-gather.2 = f32[16,1,512]{2,1,0:T(1,128)S(1)} all-gather(f32[2,1,512]{2,1,0:T(1,128)S(1)} %slice_add_fusion.19), channel_id=4, replica_groups=mesh['sp'=8,'tp'=4] {'sp'}, dimensions={0}, use_global_device_ids=true | all-gather | bytes 36864 | tf_op jit(solution)/shard_map/all_gather | solution.py:26
  169.2 31.4 %all-gather.3 = f32[16,1,512]{2,1,0:T(1,128)S(1)} all-gather(f32[2,1,512]{2,1,0:T(1,128)S(1)} %slice_add_fusion.16), channel_id=5, replica_groups=mesh['sp'=8,'tp'=4] {'sp'}, dimensions={0}, use_global_device_ids=true | all-gather | bytes 36864 | tf_op jit(solution)/shard_map/all_gather | solution.py:26
  201.5 30.6 %all-gather = f32[16,1,512]{2,1,0:T(1,128)S(1)} all-gather(f32[2,1,512]{2,1,0:T(1,128)S(1)} %slice_add_fusion.23), channel_id=2, replica_groups=mesh['sp'=8,'tp'=4] {'sp'}, dimensions={0}, use_global_device_ids=true | all-gather | bytes 36864 | tf_op jit(solution)/shard_map/all_gather | solution.py:26
  232.2 30.6 %all-gather.1 = f32[16,1,512]{2,1,0:T(1,128)S(1)} all-gather(f32[2,1,512]{2,1,0:T(1,128)S(1)} %slice_add_fusion.20), channel_id=3, replica_groups=mesh['sp'=8,'tp'=4] {'sp'}, dimensions={0}, use_global_device_ids=true | all-gather | bytes 36864 | tf_op jit(solution)/shard_map/all_gather | solution.py:26
  266.4 17.8 %reduce-scatter.4.cloned.1.call-done = bf16[32,256]{1,0:T(8,128)(2,1)} async-done(((bf16[32,1024]{1,0:T(8,128)(2,1)}), bf16[32,256]{1,0:T(8,128)(2,1)}) %reduce-scatter.4.cloned.1.call-update) | async-done | bytes 16400 | tf_op jit(solution)/shard_map/reduce_scatter | solution.py:135
  284.2 5.4 all_gather.62
  306.9 32.5 %all-gather.6 = f32[16,1,512]{2,1,0:T(1,128)S(1)} all-gather(f32[2,1,512]{2,1,0:T(1,128)S(1)} %slice_add_fusion.11), channel_id=8, replica_groups=mesh['sp'=8,'tp'=4] {'sp'}, dimensions={0}, use_global_device_ids=true | all-gather | bytes 36864 | tf_op jit(solution)/shard_map/all_gather | solution.py:26
  339.6 30.6 %all-gather.7 = f32[16,1,512]{2,1,0:T(1,128)S(1)} all-gather(f32[2,1,512]{2,1,0:T(1,128)S(1)} %slice_add_fusion.8), channel_id=9, replica_groups=mesh['sp'=8,'tp'=4] {'sp'}, dimensions={0}, use_global_device_ids=true | all-gather | bytes 36864 | tf_op jit(solution)/shard_map/all_gather | solution.py:26
  374.0 30.6 %all-gather.4 = f32[16,1,512]{2,1,0:T(1,128)S(1)} all-gather(f32[2,1,512]{2,1,0:T(1,128)S(1)} %slice_add_fusion.15), channel_id=6, replica_groups=mesh['sp'=8,'tp'=4] {'sp'}, dimensions={0}, use_global_device_ids=true | all-gather | bytes 36864 | tf_op jit(solution)/shard_map/all_gather | solution.py:26
  406.0 32.0 %all-gather.5 = f32[16,1,512]{2,1,0:T(1,128)} all-gather(f32[2,1,512]{2,1,0:T(1,128)S(1)} %slice_add_fusion.12), channel_id=7, replica_groups=mesh['sp'=8,'tp'=4] {'sp'}, dimensions={0}, use_global_device_ids=true | all-gather | bytes 36864 | tf_op jit(solution)/shard_map/all_gather | solution.py:26
  440.9 5.0 while.86
  447.7 17.9 %reduce-scatter.6.cloned.1.call-done = bf16[32,256]{1,0:T(8,128)(2,1)} async-done(((bf16[32,1024]{1,0:T(8,128)(2,1)}), bf16[32,256]{1,0:T(8,128)(2,1)}) %reduce-scatter.6.cloned.1.call-update) | async-done | bytes 16400 | tf_op jit(solution)/shard_map/reduce_scatter | solution.py:135
  465.7 5.4 all_gather.67
  474.8 4.7 collective-permute-start.4
  492.6 32.3 %all-gather.10 = f32[16,1,512]{2,1,0:T(1,128)S(1)} all-gather(f32[2,1,512]{2,1,0:T(1,128)S(1)} %slice_add_fusion.3), channel_id=12, replica_groups=mesh['sp'=8,'tp'=4] {'sp'}, dimensions={0}, use_global_device_ids=true | all-gather | bytes 36864 | tf_op jit(solution)/shard_map/all_gather | solution.py:26
  525.1 30.6 %all-gather.11 = f32[16,1,512]{2,1,0:T(1,128)S(1)} all-gather(f32[2,1,512]{2,1,0:T(1,128)S(1)} %slice_add_fusion), channel_id=13, replica_groups=mesh['sp'=8,'tp'=4] {'sp'}, dimensions={0}, use_global_device_ids=true | all-gather | bytes 36864 | tf_op jit(solution)/shard_map/all_gather | solution.py:26
  559.4 30.6 %all-gather.8 = f32[16,1,512]{2,1,0:T(1,128)S(1)} all-gather(f32[2,1,512]{2,1,0:T(1,128)S(1)} %slice_add_fusion.7), channel_id=10, replica_groups=mesh['sp'=8,'tp'=4] {'sp'}, dimensions={0}, use_global_device_ids=true | all-gather | bytes 36864 | tf_op jit(solution)/shard_map/all_gather | solution.py:26
  591.5 32.2 %all-gather.9 = f32[16,1,512]{2,1,0:T(1,128)} all-gather(f32[2,1,512]{2,1,0:T(1,128)S(1)} %slice_add_fusion.4), channel_id=11, replica_groups=mesh['sp'=8,'tp'=4] {'sp'}, dimensions={0}, use_global_device_ids=true | all-gather | bytes 36864 | tf_op jit(solution)/shard_map/all_gather | solution.py:26
  626.6 5.0 while.88
  633.3 17.8 %reduce-scatter.8.cloned.1.call-done = bf16[32,256]{1,0:T(8,128)(2,1)} async-done(((bf16[32,1024]{1,0:T(8,128)(2,1)}), bf16[32,256]{1,0:T(8,128)(2,1)}) %reduce-scatter.8.cloned.1.call-update) | async-done | bytes 16400 | tf_op jit(solution)/shard_map/reduce_scatter | solution.py:135
  (512 shorter events, 80.8 us)
Async XLA Ops:
  6.5 128.2 %copy-start.3 = (bf16[3,2,4,128,128]{4,3,2,1,0:T(8,128)(2,1)S(1)}, bf16[3,2,4,128,128]{4,3,2,1,0:T(8,128)(2,1)}, u32[]{:S(2)}) copy-start(bf16[3,2,4,128,128]{4,3,2,1,0:T(8,128)(2,1)} %param.26) | copy-start | bytes 2359300
  6.5 128.6 %copy-start.4 = (bf16[3,2,4,128,128]{4,3,2,1,0:T(8,128)(2,1)S(1)}, bf16[3,2,4,128,128]{4,3,2,1,0:T(8,128)(2,1)}, u32[]{:S(2)}) copy-start(bf16[3,2,4,128,128]{4,3,2,1,0:T(8,128)(2,1)} %param.25) | copy-start | bytes 2359300
  6.5 65.8 %all-gather.16.cloned.1.call-start = ((), (), s32[]{:S(2)}) async-start(), calls=%async_computation.3 | async-start | bytes 3538944 | tf_op jit(solution)/shard_map/all_gather | solution.py:62
  7.3 125.9 %all-gather.18.cloned.1.call-start = ((), (), s32[]{:S(2)}) async-start(), calls=%async_computation.4 | async-start | bytes 3538944 | tf_op jit(solution)/shard_map/all_gather | solution.py:63
  8.0 255.6 %all-gather.20.cloned.1.call-start = ((), (), s32[]{:S(2)}) async-start(), calls=%async_computation.5 | async-start | bytes 3538944 | tf_op jit(solution)/shard_map/all_gather | solution.py:65
  8.7 275.5 %reduce-scatter.4.cloned.1.call-start = ((), (), s32[]{:S(2)}) async-start(), calls=%async_computation.6 | async-start | bytes 81920 | tf_op jit(solution)/shard_map/reduce_scatter | solution.py:135
  73.8 60.9 %collective-permute-start.1 = (bf16[2,2,512]{2,1,0:T(2,128)(2,1)S(1)}, bf16[2,2,512]{2,1,0:T(2,128)(2,1)S(1)}, u32[]{:S(2)}, u32[]{:S(2)}) collective-permute-start(bf16[2,2,512]{2,1,0:T(2,128)(2,1)S(1)} %get-tuple-element.783), channel_id=1, source_target_pairs={{4,0},{8,4},{12,8},{16,12},{20,16},{24,20},{28,24},{5,1},{9,5},{13... | collective-permute-start | bytes 12296 | tf_op jit(solution)/shard_map/ppermute | solution.py:19
  75.1 59.6 %collective-permute-start = (bf16[2,2,512]{2,1,0:T(2,128)(2,1)S(1)}, bf16[2,2,512]{2,1,0:T(2,128)(2,1)S(1)}, u32[]{:S(2)}, u32[]{:S(2)}) collective-permute-start(bf16[2,2,512]{2,1,0:T(2,128)(2,1)S(1)} %get-tuple-element.784), channel_id=1, source_target_pairs={{0,4},{4,8},{8,12},{12,16},{16,20},{20,24},{24,28},{1,5},{5,9},{9,... | collective-permute-start | bytes 12296 | tf_op jit(solution)/shard_map/ppermute | solution.py:18
  265.8 199.9 %reduce-scatter.6.cloned.1.call-start = ((), (), s32[]{:S(2)}) async-start(), calls=%async_computation.7 | async-start | bytes 81920 | tf_op jit(solution)/shard_map/reduce_scatter | solution.py:135
  291.4 8.0 %collective-permute-start.3 = (bf16[2,2,512]{2,1,0:T(2,128)(2,1)S(1)}, bf16[2,2,512]{2,1,0:T(2,128)(2,1)S(1)}, u32[]{:S(2)}, u32[]{:S(2)}) collective-permute-start(bf16[2,2,512]{2,1,0:T(2,128)(2,1)S(1)} %get-tuple-element.773), channel_id=1, source_target_pairs={{4,0},{8,4},{12,8},{16,12},{20,16},{24,20},{28,24},{5,1},{9,5},{13... | collective-permute-start | bytes 12296 | tf_op jit(solution)/shard_map/ppermute | solution.py:19
  292.7 6.7 %collective-permute-start.2 = (bf16[2,2,512]{2,1,0:T(2,128)(2,1)S(1)}, bf16[2,2,512]{2,1,0:T(2,128)(2,1)S(1)}, u32[]{:S(2)}, u32[]{:S(2)}) collective-permute-start(bf16[2,2,512]{2,1,0:T(2,128)(2,1)S(1)} %get-tuple-element.774), channel_id=1, source_target_pairs={{0,4},{4,8},{8,12},{12,16},{16,20},{20,24},{24,28},{1,5},{5,9},{9,... | collective-permute-start | bytes 12296 | tf_op jit(solution)/shard_map/ppermute | solution.py:18
  301.8 144.9 %copy-start = (bf16[3,512,1024]{2,1,0:T(8,128)(2,1)S(1)}, bf16[3,512,1024]{2,1,0:T(8,128)(2,1)}, u32[]{:S(2)}) copy-start(bf16[3,512,1024]{2,1,0:T(8,128)(2,1)} %all-gather.20.cloned.1.call-done) | copy-start | bytes 9437188
  370.9 110.8 %copy-start.2 = (f32[1,1,512]{2,1,0:T(1,128)S(1)}, f32[1,1,512]{2,1,0:T(1,128)}, u32[]{:S(2)}) copy-start(f32[1,1,512]{2,1,0:T(1,128)} %get-tuple-element.857) | copy-start | bytes 6148
  405.3 80.4 %copy-start.1 = (f32[1,1,512]{2,1,0:T(1,128)S(1)}, f32[1,1,512]{2,1,0:T(1,128)}, u32[]{:S(2)}) copy-start(f32[1,1,512]{2,1,0:T(1,128)} %get-tuple-element.841) | copy-start | bytes 6148
  447.7 203.4 %reduce-scatter.8.cloned.1.call-start = ((), (), s32[]{:S(2)}) async-start(), calls=%async_computation.8 | async-start | bytes 81920 | tf_op jit(solution)/shard_map/reduce_scatter | solution.py:135
  473.5 8.2 %collective-permute-start.5 = (bf16[2,2,512]{2,1,0:T(2,128)(2,1)S(1)}, bf16[2,2,512]{2,1,0:T(2,128)(2,1)S(1)}, u32[]{:S(2)}, u32[]{:S(2)}) collective-permute-start(bf16[2,2,512]{2,1,0:T(2,128)(2,1)S(1)} %get-tuple-element.763), channel_id=1, source_target_pairs={{4,0},{8,4},{12,8},{16,12},{20,16},{24,20},{28,24},{5,1},{9,5},{13... | collective-permute-start | bytes 12296 | tf_op jit(solution)/shard_map/ppermute | solution.py:19
  474.8 6.9 %collective-permute-start.4 = (bf16[2,2,512]{2,1,0:T(2,128)(2,1)S(1)}, bf16[2,2,512]{2,1,0:T(2,128)(2,1)S(1)}, u32[]{:S(2)}, u32[]{:S(2)}) collective-permute-start(bf16[2,2,512]{2,1,0:T(2,128)(2,1)S(1)} %get-tuple-element.764), channel_id=1, source_target_pairs={{0,4},{4,8},{8,12},{12,16},{16,20},{20,24},{24,28},{1,5},{5,9},{9,... | collective-permute-start | bytes 12296 | tf_op jit(solution)/shard_map/ppermute | solution.py:18
Sparse Core Ops, SparseCore 0:
  9.5 62.7 all-gather.15
  74.5 58.6 all-gather.17
  135.2 62.0 all-gather.19
  265.9 18.3 reduce-scatter.3
  447.8 17.8 reduce-scatter.5
  633.4 17.6 reduce-scatter.7
where the time goes:
time: 660 us; the launch traced here: 658 us
  blocking collectives  392 us (59%)
  waiting for transfers between devices  162 us (25%)
  other arithmetic  28.7 us (4%)
  matrix products  20.8 us (3%)
  local copies, waits for them, and re-layouts  19.3 us (3%)
  starting transfers between devices  17.9 us (3%)
  between operations  15.6 us (2%)
    all_gather x12, blocking collectives, carried_in(): pieces = jax.tree.map(lambda part: lax.all_gather(part, axis), value)  375 us
    all_gather x1, waiting for transfers between devices, body(): lax.all_gather(gate_weight, 'sp', axis=1, tiled=True)  53.5 us
    reduce_scatter x3, waiting for transfers between devices, body(): lax.psum_scatter(partial_terms.astype(jnp.bfloat16), 'tp', scatter_dimens...  53.5 us
    all_gather x1, waiting for transfers between devices, body(): lax.all_gather(in_weight, 'sp', axis=1, tiled=True)  53.2 us
    all_gather x3, blocking collectives, body(): gathered = lax.all_gather(state, 'tp', axis=2, tiled=True)  17.3 us
    ppermute x3, starting transfers between devices, extended(): before = lax.ppermute(last, axis, up)  13.8 us
  transfers between devices with their start and end apart: 12, of which 5 were waited for; matrix products, arithmetic and copies ran while one was open for 2% of the time, Pallas kernels for 0%

commit v1 on v0

--- a/solution.py
+++ b/solution.py
@@ -59,7 +59,7 @@
     seq_len = tok_rows * lax.axis_size("sp")
     chan_width = in_weight.shape[2]
     in_whole, gate_whole = (
-        lax.all_gather(in_weight, "sp", axis=1, tiled=True),
+        jnp.concatenate(lax.all_gather(in_weight, "sp"), axis=1),
         lax.all_gather(gate_weight, "sp", axis=1, tiled=True),
     )
     out_whole = lax.all_gather(out_weight, "sp", axis=2, tiled=True)

time: 660 us -> 626 us (0.948)
  other arithmetic: 28.7 us -> 6.11 us
  local copies, waits for them, and re-layouts: 19.3 us -> 10.1 us
  waiting for transfers between devices: 162 us -> 171 us
    select_n x42, other arithmetic: 10.3 us -> 0.73 us  [hop(): jnp.where(position < mine, new, old)]
  transfers between devices with their start and end apart: 12 -> 12, of which waited for: 5 -> 7; matrix products, arithmetic and copies ran while one was open for 2% -> 3% of each run, Pallas kernels for 0% -> 0%
where the time goes in v1:
time: 626 us
  blocking collectives  386 us (62%)
  waiting for transfers between devices  171 us (27%)
  matrix products  21.9 us (3%)
  between operations  15.8 us (3%)
  starting transfers between devices  13.5 us (2%)
  local copies, waits for them, and re-layouts  10.1 us (2%)
    all_gather x12, blocking collectives, carried_in(): pieces = jax.tree.map(lambda part: lax.all_gather(part, axis), value)  369 us
    all_gather x1, waiting for transfers between devices, body(): lax.all_gather(gate_weight, 'sp', axis=1, tiled=True)  54.7 us
    reduce_scatter x3, waiting for transfers between devices, body(): lax.psum_scatter(partial_terms.astype(jnp.bfloat16), 'tp', scatter_dimens...  54.5 us
    all_gather x1, waiting for transfers between devices, body(): lax.all_gather(in_weight, 'sp')  54.4 us
    all_gather x3, blocking collectives, body(): gathered = lax.all_gather(state, 'tp', axis=2, tiled=True)  17.3 us
  transfers between devices with their start and end apart: 12, of which 7 were waited for; matrix products, arithmetic and copies ran while one was open for 3% of the time, Pallas kernels for 0%

profile of v1, /device:TPU:0, one launch (start us, length us, event | category | flops | bytes accessed | tf_op | source)
XLA Modules:
  0.0 625.6 jit_solution(13598644998536827367)
XLA Ops:
  9.7 6.5 %all_gather.57 = bf16[2,16,1024]{2,1,0:T(8,128)(2,1)S(1)} all-gather(bf16[2,16,256]{2,1,0:T(8,128)(2,1)} %param.21), channel_id=1, replica_groups=mesh['sp'=8,'tp'=4] {'tp'}, dimensions={2}, use_global_device_ids=true | all-gather | bytes 81920 | tf_op jit(solution)/shard_map/all_gather | solution.py:68
  17.9 54.4 %all-gather.21.cloned.1.call-done = bf16[24,128,512]{2,1,0:T(8,128)(2,1)} async-done(((bf16[3,128,512]{2,1,0:T(8,128)(2,1)}), bf16[24,128,512]{2,1,0:T(8,128)(2,1)}) %all-gather.21.cloned.1.call-update) | async-done | bytes 3145744 | tf_op jit(solution)/shard_map/all_gather | solution.py:62
  78.5 54.7 %all-gather.17.cloned.1.call-done = bf16[3,1024,512]{2,1,0:T(8,128)(2,1)} async-done(((bf16[3,128,512]{2,1,0:T(8,128)(2,1)}), bf16[3,1024,512]{2,1,0:T(8,128)(2,1)}) %all-gather.17.cloned.1.call-update) | async-done | bytes 3145744 | tf_op jit(solution)/shard_map/all_gather | solution.py:63
  141.3 31.3 %all-gather.2 = f32[16,1,512]{2,1,0:T(1,128)S(1)} all-gather(f32[2,1,512]{2,1,0:T(1,128)S(1)} %slice_add_fusion.20), channel_id=4, replica_groups=mesh['sp'=8,'tp'=4] {'sp'}, dimensions={0}, use_global_device_ids=true | all-gather | bytes 36864 | tf_op jit(solution)/shard_map/all_gather | solution.py:26
  172.8 31.3 %all-gather.1 = f32[16,1,512]{2,1,0:T(1,128)S(1)} all-gather(f32[2,1,512]{2,1,0:T(1,128)S(1)} %slice_add_fusion.23), channel_id=3, replica_groups=mesh['sp'=8,'tp'=4] {'sp'}, dimensions={0}, use_global_device_ids=true | all-gather | bytes 36864 | tf_op jit(solution)/shard_map/all_gather | solution.py:26
  205.1 30.6 %all-gather.4 = f32[16,1,512]{2,1,0:T(1,128)S(1)} all-gather(f32[2,1,512]{2,1,0:T(1,128)S(1)} %slice_add_fusion.16), channel_id=6, replica_groups=mesh['sp'=8,'tp'=4] {'sp'}, dimensions={0}, use_global_device_ids=true | all-gather | bytes 36864 | tf_op jit(solution)/shard_map/all_gather | solution.py:26
  235.9 30.6 %all-gather.3 = f32[16,1,512]{2,1,0:T(1,128)S(1)} all-gather(f32[2,1,512]{2,1,0:T(1,128)S(1)} %slice_add_fusion.19), channel_id=5, replica_groups=mesh['sp'=8,'tp'=4] {'sp'}, dimensions={0}, use_global_device_ids=true | all-gather | bytes 36864 | tf_op jit(solution)/shard_map/all_gather | solution.py:26
  269.9 18.1 %reduce-scatter.4.cloned.1.call-done = bf16[32,256]{1,0:T(8,128)(2,1)} async-done(((bf16[32,1024]{1,0:T(8,128)(2,1)}), bf16[32,256]{1,0:T(8,128)(2,1)}) %reduce-scatter.4.cloned.1.call-update) | async-done | bytes 16400 | tf_op jit(solution)/shard_map/reduce_scatter | solution.py:135
  288.0 5.4 all_gather.66
  293.9 3.4 collective-permute-start.2
  300.1 2.7 collective-permute-done.3
  309.4 30.7 %all-gather.6 = f32[16,1,512]{2,1,0:T(1,128)S(1)} all-gather(f32[2,1,512]{2,1,0:T(1,128)S(1)} %slice_add_fusion.12), channel_id=8, replica_groups=mesh['sp'=8,'tp'=4] {'sp'}, dimensions={0}, use_global_device_ids=true | all-gather | bytes 36864 | tf_op jit(solution)/shard_map/all_gather | solution.py:26
  340.3 30.6 %all-gather.5 = f32[16,1,512]{2,1,0:T(1,128)S(1)} all-gather(f32[2,1,512]{2,1,0:T(1,128)S(1)} %slice_add_fusion.15), channel_id=7, replica_groups=mesh['sp'=8,'tp'=4] {'sp'}, dimensions={0}, use_global_device_ids=true | all-gather | bytes 36864 | tf_op jit(solution)/shard_map/all_gather | solution.py:26
  371.4 30.6 %all-gather.8 = f32[16,1,512]{2,1,0:T(1,128)S(1)} all-gather(f32[2,1,512]{2,1,0:T(1,128)S(1)} %slice_add_fusion.8), channel_id=10, replica_groups=mesh['sp'=8,'tp'=4] {'sp'}, dimensions={0}, use_global_device_ids=true | all-gather | bytes 36864 | tf_op jit(solution)/shard_map/all_gather | solution.py:26
  402.1 30.6 %all-gather.7 = f32[16,1,512]{2,1,0:T(1,128)S(1)} all-gather(f32[2,1,512]{2,1,0:T(1,128)S(1)} %slice_add_fusion.11), channel_id=9, replica_groups=mesh['sp'=8,'tp'=4] {'sp'}, dimensions={0}, use_global_device_ids=true | all-gather | bytes 36864 | tf_op jit(solution)/shard_map/all_gather | solution.py:26
  435.6 18.1 %reduce-scatter.6.cloned.1.call-done = bf16[32,256]{1,0:T(8,128)(2,1)} async-done(((bf16[32,1024]{1,0:T(8,128)(2,1)}), bf16[32,256]{1,0:T(8,128)(2,1)}) %reduce-scatter.6.cloned.1.call-update) | async-done | bytes 16400 | tf_op jit(solution)/shard_map/reduce_scatter | solution.py:135
  453.7 5.4 all_gather.71
  459.6 3.4 collective-permute-start.4
  466.0 2.5 collective-permute-done.5
  474.3 30.7 %all-gather.10 = f32[16,1,512]{2,1,0:T(1,128)S(1)} all-gather(f32[2,1,512]{2,1,0:T(1,128)S(1)} %slice_add_fusion.4), channel_id=12, replica_groups=mesh['sp'=8,'tp'=4] {'sp'}, dimensions={0}, use_global_device_ids=true | all-gather | bytes 36864 | tf_op jit(solution)/shard_map/all_gather | solution.py:26
  505.2 30.6 %all-gather.9 = f32[16,1,512]{2,1,0:T(1,128)S(1)} all-gather(f32[2,1,512]{2,1,0:T(1,128)S(1)} %slice_add_fusion.7), channel_id=11, replica_groups=mesh['sp'=8,'tp'=4] {'sp'}, dimensions={0}, use_global_device_ids=true | all-gather | bytes 36864 | tf_op jit(solution)/shard_map/all_gather | solution.py:26
  536.2 30.6 %all-gather.12 = f32[16,1,512]{2,1,0:T(1,128)S(1)} all-gather(f32[2,1,512]{2,1,0:T(1,128)S(1)} %slice_add_fusion), channel_id=14, replica_groups=mesh['sp'=8,'tp'=4] {'sp'}, dimensions={0}, use_global_device_ids=true | all-gather | bytes 36864 | tf_op jit(solution)/shard_map/all_gather | solution.py:26
  566.9 30.6 %all-gather.11 = f32[16,1,512]{2,1,0:T(1,128)S(1)} all-gather(f32[2,1,512]{2,1,0:T(1,128)S(1)} %slice_add_fusion.3), channel_id=13, replica_groups=mesh['sp'=8,'tp'=4] {'sp'}, dimensions={0}, use_global_device_ids=true | all-gather | bytes 36864 | tf_op jit(solution)/shard_map/all_gather | solution.py:26
  600.4 18.3 %reduce-scatter.8.cloned.1.call-done = bf16[32,256]{1,0:T(8,128)(2,1)} async-done(((bf16[32,1024]{1,0:T(8,128)(2,1)}), bf16[32,256]{1,0:T(8,128)(2,1)}) %reduce-scatter.8.cloned.1.call-update) | async-done | bytes 16400 | tf_op jit(solution)/shard_map/reduce_scatter | solution.py:135
  (505 shorter events, 48.8 us)
Async XLA Ops:
  6.5 65.7 %all-gather.21.cloned.1.call-start = ((), (), s32[]{:S(2)}) async-start(), calls=%async_computation.8 | async-start | bytes 3538944 | tf_op jit(solution)/shard_map/all_gather | solution.py:62
  7.3 125.9 %all-gather.17.cloned.1.call-start = ((), (), s32[]{:S(2)}) async-start(), calls=%async_computation.3 | async-start | bytes 3538944 | tf_op jit(solution)/shard_map/all_gather | solution.py:63
  8.0 259.5 %all-gather.19.cloned.1.call-start = ((), (), s32[]{:S(2)}) async-start(), calls=%async_computation.4 | async-start | bytes 3538944 | tf_op jit(solution)/shard_map/all_gather | solution.py:65
  8.7 279.2 %reduce-scatter.4.cloned.1.call-start = ((), (), s32[]{:S(2)}) async-start(), calls=%async_computation.5 | async-start | bytes 81920 | tf_op jit(solution)/shard_map/reduce_scatter | solution.py:135
  74.7 60.0 %collective-permute-start = (bf16[2,2,512]{2,1,0:T(2,128)(2,1)S(1)}, bf16[2,2,512]{2,1,0:T(2,128)(2,1)S(1)}, u32[]{:S(2)}, u32[]{:S(2)}) collective-permute-start(bf16[2,2,512]{2,1,0:T(2,128)(2,1)S(1)} %get-tuple-element.787), channel_id=1, source_target_pairs={{0,4},{4,8},{8,12},{12,16},{16,20},{20,24},{24,28},{1,5},{5,9},{9,... | collective-permute-start | bytes 12296 | tf_op jit(solution)/shard_map/ppermute | solution.py:18
  77.2 57.5 %collective-permute-start.1 = (bf16[2,2,512]{2,1,0:T(2,128)(2,1)S(1)}, bf16[2,2,512]{2,1,0:T(2,128)(2,1)S(1)}, u32[]{:S(2)}, u32[]{:S(2)}) collective-permute-start(bf16[2,2,512]{2,1,0:T(2,128)(2,1)S(1)} %get-tuple-element.786), channel_id=1, source_target_pairs={{4,0},{8,4},{12,8},{16,12},{20,16},{24,20},{28,24},{5,1},{9,5},{13... | collective-permute-start | bytes 12296 | tf_op jit(solution)/shard_map/ppermute | solution.py:19
  267.5 39.2 %copy-start = (bf16[3,2,4,128,128]{4,3,2,1,0:T(8,128)(2,1)S(1)}, bf16[3,2,4,128,128]{4,3,2,1,0:T(8,128)(2,1)}, u32[]{:S(2)}) copy-start(bf16[3,2,4,128,128]{4,3,2,1,0:T(8,128)(2,1)} %param.25) | copy-start | bytes 2359300
  269.8 183.9 %reduce-scatter.6.cloned.1.call-start = ((), (), s32[]{:S(2)}) async-start(), calls=%async_computation.6 | async-start | bytes 81920 | tf_op jit(solution)/shard_map/reduce_scatter | solution.py:135
  293.9 6.2 collective-permute-start.2
  297.3 5.5 collective-permute-start.3
  435.6 183.1 %reduce-scatter.8.cloned.1.call-start = ((), (), s32[]{:S(2)}) async-start(), calls=%async_computation.7 | async-start | bytes 81920 | tf_op jit(solution)/shard_map/reduce_scatter | solution.py:135
  459.6 6.4 %collective-permute-start.4 = (bf16[2,2,512]{2,1,0:T(2,128)(2,1)S(1)}, bf16[2,2,512]{2,1,0:T(2,128)(2,1)S(1)}, u32[]{:S(2)}, u32[]{:S(2)}) collective-permute-start(bf16[2,2,512]{2,1,0:T(2,128)(2,1)S(1)} %get-tuple-element.767), channel_id=1, source_target_pairs={{0,4},{4,8},{8,12},{12,16},{16,20},{20,24},{24,28},{1,5},{5,9},{9,... | collective-permute-start | bytes 12296 | tf_op jit(solution)/shard_map/ppermute | solution.py:18
  463.0 5.5 collective-permute-start.5
Sparse Core Ops, SparseCore 0:
  9.5 62.7 all-gather.20
  74.5 58.6 all-gather.16
  135.2 62.0 all-gather.18
  269.9 17.9 reduce-scatter.3
  435.7 17.9 reduce-scatter.5
  600.5 18.1 reduce-scatter.7
